TPU v7x, 32 devices: a whole 2x2x4 slice. The times are simulated.
32 devices in a mesh: sp: 16 (over z, y, x), tp: 2 (over core).
Axes of the slice: x: 2, y: 2, z: 4, core: 2. Of those that a mesh axis runs over, the one named last changes fastest.
Arguments:
- tokens: bfloat16 [4608, 4096], P('sp', 'tp'), may hold values from -6 to 6
- doc_ids: int32 [4608], P('sp'), may hold values from 0 to 3, never falling along the last dimension, each value on 1 to 2304 neighbouring positions
- norm_gain: float32 [2, 4096], replicated, may hold values from 0.1 to 1.9
- in_proj: bfloat16 [2, 4096, 4096], P(None, 'sp', 'tp'), may hold values from -0.09375 to 0.09375
- mix_proj: bfloat16 [2, 1024, 4096], P(None, 'sp', 'tp'), may hold values from -0.1875 to 0.1875
- out_scale: float32 [2, 4096], replicated, may hold values from 0.1 to 1.9
Outputs:
- mixed_out: bfloat16 [4608, 4096], P('sp', 'tp')
Inputs may be any that keep to these rules, and one draw needn't show every extreme that they name: `doc_ids`: document numbers never fall along the sequence, run from 0 to 3, and each document holds at most 2304 positions.
All inputs are finite; a program needn't handle non-finite values.
Results may differ from a plain program's by a relative error of at most 0.0085.
Values may be sent and summed in bfloat16 or wider, within the bound.
A program may use at most 128 MiB of HBM per device.

v0:
```python
import functools

import jax
import jax.numpy as jnp
from jax import lax
from jax.experimental import pallas as pl
from jax.experimental.pallas import tpu as pltpu
from jax.sharding import PartitionSpec as P

D = 4096
WIN = 16
LAYERS = 2
HALO = LAYERS * WIN


epsilon = 1e-06


def from_behind(block, axis, distance):
    devices = range(lax.axis_size(axis))
    route = [(i - distance, i) for i in devices if i - distance in devices]
    return lax.ppermute(block, axis, route)


def partner_2(value, axis, stride):
    mask = 2**stride
    pairs = [(source, source ^ mask) for source in range(lax.axis_size(axis))]
    return lax.ppermute(value, axis, pairs)


def normalize(current, gain_row):
    values = current.astype(jnp.float32)
    scaled = values * lax.rsqrt(jnp.mean(values * values, axis=-1, keepdims=True) + epsilon)
    return (scaled * gain_row[None, :]).astype(jnp.bfloat16)


def pool_block(extended, ext_flags, own_flags, proj_f32, windows, local_rows):
    window_sum = jnp.zeros_like(proj_f32)
    window_count = jnp.zeros_like(proj_f32)
    for offset in range(WIN):
        begin = WIN - 1 - offset
        shifted = extended[begin : begin + local_rows]
        same_doc = ext_flags[begin : begin + local_rows] == own_flags
        taken = same_doc[:, None] & (offset < windows)[None, :]
        window_sum = window_sum + jnp.where(taken, shifted, jnp.float32(0.0))
        window_count = window_count + taken.astype(jnp.float32)
    return (window_sum / window_count - proj_f32).astype(jnp.bfloat16)


def shards(tokens, doc_ids, norm_gain, in_proj, mix_proj, out_scale):
    local_rows = tokens.shape[0]
    local_width = tokens.shape[1]
    block_width = D // 8
    blocks_here = local_width // block_width
    tp_count = lax.axis_size("tp")
    half_bit = tp_count.bit_length() - 2
    tp_index = lax.axis_index("tp")
    chan_start = tp_index * local_width
    channels = chan_start + jnp.arange(local_width, dtype=jnp.int32)
    windows = jnp.left_shift(jnp.int32(2), channels // block_width % 4)
    low_side = tp_index < tp_count // 2
    doc_flags = (doc_ids + 1).astype(jnp.bfloat16)
    in_whole, mix_whole = (
        lax.all_gather(in_proj, "sp", axis=1, tiled=True),
        lax.all_gather(mix_proj, "sp", axis=1, tiled=True),
    )
    current = tokens
    for depth_idx in range(LAYERS):
        gathered = lax.all_gather(current, "tp", axis=1, tiled=True)
        normed = normalize(gathered, norm_gain[depth_idx])
        proj_sum = jnp.dot(normed, in_whole[depth_idx], preferred_element_type=jnp.float32)
        projected = proj_sum.astype(jnp.bfloat16)
        tail_rows, tail_flags = from_behind(
            (projected[local_rows - (WIN - 1) :], doc_flags[local_rows - (WIN - 1) :]), "sp", 1
        )
        extended = jnp.concatenate([tail_rows, projected], axis=0).astype(jnp.float32)
        ext_flags = jnp.concatenate([tail_flags, doc_flags], axis=0)
        pooled = pool_block(
            extended, ext_flags, doc_flags, projected.astype(jnp.float32), windows, local_rows
        )
        partner = partner_2(pooled, "tp", half_bit)
        low_part = jnp.where(low_side, pooled, partner)
        high_part = jnp.where(low_side, partner, pooled)
        group_inputs = [
            jnp.concatenate(
                [
                    low_part[:, block_idx * block_width : (block_idx + 1) * block_width],
                    high_part[:, block_idx * block_width : (block_idx + 1) * block_width],
                ],
                axis=1,
            )
            for block_idx in range(blocks_here)
        ]
        shard_rows = mix_whole[depth_idx]
        pieces_out = []
        for add_block_idx in range(blocks_here):
            add_inputs = group_inputs[add_block_idx]
            pieces_out.append(
                jnp.dot(
                    add_inputs,
                    shard_rows[:, add_block_idx * block_width : (add_block_idx + 1) * block_width],
                    preferred_element_type=jnp.float32,
                )
            )
        grouped = jnp.concatenate(pieces_out, axis=1)
        scale_row = lax.dynamic_slice_in_dim(out_scale[depth_idx], chan_start, local_width, 0)
        current = (grouped * scale_row[None, :]).astype(jnp.bfloat16)
    return current


def peer_of(g, k):
    return (g // 2 + k // 2) % 2 * 2 + (g % 2 + k % 2) % 2


def fused_kernel(
    nz, own, tok, in_w, mix_w, gain, scale, out,
    xt, normed, acts, w_in, w_mix, acc, proj, docs, pooled, last,
    rx_in, rx_mix, up_in, up_mix, dn_in, dn_mix, tx_in, tx_mix,
    tok_rx, tok_prx, tok_tx, tok_ptx, halo, halo_tx, act_rx, act_prx, act_tx, act_ptx,
    pool_sem, out_rx, out_tx,
):
    sp = lax.axis_index("sp")
    c = lax.axis_index("tp")
    z, g = sp // 4, sp % 4
    total = HALO + 4 * own
    width = w_in.shape[2]
    k_in, k_mix = in_w.shape[1], mix_w.shape[1]
    partner = (sp, 1 - c)

    def peer(k):
        return (z * 4 + peer_of(g, k), c)

    def remote(src, dst, tx, rx, to):
        return pltpu.make_async_remote_copy(
            src_ref=src, dst_ref=dst, send_sem=tx, recv_sem=rx, device_id=to,
            device_id_type=pl.DeviceIdType.MESH,
        )

    barrier = pltpu.get_barrier_semaphore()

    def greet(to):
        pl.semaphore_signal(barrier, inc=1, device_id=to, device_id_type=pl.DeviceIdType.MESH)

    for k in (1, 2, 3):
        greet(peer(k))
    greet(partner)

    @pl.when(z > 0)
    def _():
        greet((sp - 4, c))

    @pl.when(z < nz - 1)
    def _():
        greet((sp + 4, c))

    ends = jnp.where(z > 0, 1, 0) + jnp.where(z < nz - 1, 1, 0)
    pl.semaphore_wait(barrier, 4 + ends)

    def in_piece(l, s):
        return w_in.at[l, pl.ds(s * k_in, k_in), :]

    def mix_piece(l, s):
        return w_mix.at[l, pl.ds(s * k_mix, k_mix), :]

    kinds = {
        "in": (in_piece, in_w, rx_in, up_in, dn_in, tx_in),
        "mix": (mix_piece, mix_w, rx_mix, up_mix, dn_mix, tx_mix),
    }

    def own_weight(kind, l):
        piece, src, rx = kinds[kind][:3]
        return pltpu.make_async_copy(
            src.at[l, :, pl.ds(g * width, width)], piece(l, sp), rx.at[l, sp]
        )

    def give_weight(kind, l, k):
        piece, src, rx, _, _, tx = kinds[kind]
        return remote(
            src.at[l, :, pl.ds(peer_of(g, k) * width, width)], piece(l, sp),
            tx.at[l, k], rx.at[l, sp], peer(k),
        )

    def relay(kind, l, s, up):
        piece, _, rx, up_tx, dn_tx, _ = kinds[kind]
        tx = up_tx if up else dn_tx
        to = sp + 4 if up else sp - 4
        return remote(piece(l, s), piece(l, s), tx.at[l, s], rx.at[l, s], (to, c))

    def arrived(kind, l, s):
        piece, _, rx = kinds[kind][:3]
        remote(piece(l, s), piece(l, s), rx.at[l, s], rx.at[l, s], partner).wait_recv()

    def send_relay(kind, l, s, up):
        @pl.when((z < nz - 1) if up else (z > 0))
        def _():
            relay(kind, l, s, up).start()

    def pump_plane(kind, l):
        own_weight(kind, l).wait()
        send_relay(kind, l, sp, True)
        send_relay(kind, l, sp, False)
        for k in (1, 2, 3):
            s = z * 4 + peer_of(g, k)
            arrived(kind, l, s)
            send_relay(kind, l, s, True)
            send_relay(kind, l, s, False)

    def pump_far(kind, l, far, ks=range(4)):
        for k in ks:
            @pl.when(z >= far)
            def _():
                s = (z - far) * 4 + peer_of(g, k)
                arrived(kind, l, s)
                send_relay(kind, l, s, True)

            @pl.when(z + far < nz)
            def _():
                s = (z + far) * 4 + peer_of(g, k)
                arrived(kind, l, s)
                send_relay(kind, l, s, False)

    def pump_line(kind, l):
        for far in range(1, nz):
            pump_far(kind, l, far)

    def start_weights(kind, l):
        own_weight(kind, l).start()
        for k in (1, 2, 3):
            give_weight(kind, l, k).start()

    def rows_of(q):
        return pl.ds(HALO + q * own, own)

    halo_here = xt.at[c, pl.ds(0, HALO), :]
    tail = tok.at[pl.ds(own - HALO, HALO), :]
    halo_up = remote(tail, halo_here, halo_tx.at[0], halo.at[0], (sp + 4, c))
    halo_peer = {k: remote(halo_here, halo_here, halo_tx.at[k], halo.at[0], peer(k)) for k in (1, 2, 3)}
    halo_part = remote(halo_here, halo_here, halo_tx.at[4], halo.at[1], partner)

    @pl.when((z < nz - 1) & (g == 3))
    def _():
        halo_up.start()

    start_weights("in", 0)
    tok_here = pltpu.make_async_copy(tok, xt.at[c, rows_of(g), :], tok_rx.at[0])
    tok_here.start()
    tok_sent = [remote(tok, xt.at[c, rows_of(g), :], tok_ptx.at[0], tok_prx.at[0], partner)]
    for k in (1, 2):
        tok_sent.append(
            remote(tok, xt.at[c, rows_of(g), :], tok_tx.at[k], tok_rx.at[k], peer(k))
        )
    for copy in tok_sent:
        copy.start()

    @pl.when(z == 0)
    def _():
        xt[:, 0:HALO, :] = jnp.zeros((2, HALO, xt.shape[2]), xt.dtype)

    docs[0:16, :] = jnp.zeros((16, 128), jnp.float32)
    proj[0:16, :] = jnp.zeros((16, width), proj.dtype)

    def spread(block, rx, tx, prx, ptx, sent):
        for k in (1, 2):
            spot = block(c, peer_of(g, k))
            remote(spot, spot, rx.at[k], rx.at[k], partner).wait_recv()
        for k in (1, 2):
            part = half_of(block(c, peer_of(g, k)), k)
            copy = remote(part, part, tx.at[2 + k], rx.at[2 + k], peer(3 - k))
            copy.start()
            sent.append(copy)
        for k in (1, 2):
            spot = block(c, peer_of(g, k))
            copy = remote(spot, spot, ptx.at[k], prx.at[k], partner)
            copy.start()
            sent.append(copy)

    def spread_end(block, rx, prx, ptx, sent):
        spot = block(c, peer_of(g, 3))
        for k in (1, 2):
            part = half_of(spot, k)
            remote(part, part, rx.at[2 + k], rx.at[2 + k], partner).wait_recv()
        copy = remote(spot, spot, ptx.at[3], prx.at[3], partner)
        copy.start()
        sent.append(copy)

    def from_partner(block, prx, k):
        spot = block(1 - c, peer_of(g, k))
        remote(spot, spot, prx.at[k], prx.at[k], partner).wait_recv()

    def half_of(spot, k):
        n = spot.shape[0] // 2
        return spot.at[pl.ds((k - 1) * n, n), :]

    def tok_block(side, q):
        return xt.at[side, rows_of(q), :]

    half = 4 * width
    step = 16
    tile = total // 2
    chunk = 32

    def normalize_rows(l, load, start, count):
        def body(i, carry):
            r = pl.ds(pl.multiple_of(start + i * step, step), step)
            squares = jnp.zeros((step, 128), jnp.float32)
            for j in range(8):
                v = load(j, r).astype(jnp.float32)
                v = v * v
                for q in range(width // 128):
                    squares = squares + v[:, q * 128 : (q + 1) * 128]
            mean = jnp.sum(squares, axis=-1, keepdims=True) * (1.0 / (8 * width))
            factor = lax.rsqrt(mean + epsilon)
            for j in range(8):
                v = load(j, r).astype(jnp.float32) * factor
                normed[r, j * width : (j + 1) * width] = (
                    v * gain[l : l + 1, j * width : (j + 1) * width]
                ).astype(jnp.bfloat16)
            return carry

        lax.fori_loop(0, count // step, body, 0)

    def load_tokens(j, r):
        h = j // 4
        return xt[h, r, (j % 4) * width : (j % 4 + 1) * width]

    def load_acts(j, r):
        return acts[j, r, :]

    def project(l):
        for m in range(2):
            r = slice(m * tile, (m + 1) * tile)

            def body(i, carry):
                ks = pl.ds(pl.multiple_of(i * width, width), width)
                acc[r, :] += jnp.dot(
                    normed[r, ks], w_in[l, ks, :], preferred_element_type=jnp.float32
                )
                return carry

            acc[r, :] = jnp.dot(
                normed[r, 0:width], w_in[l, 0:width, :], preferred_element_type=jnp.float32
            )
            lax.fori_loop(1, 8, body, 0)
            proj[16 + m * tile : 16 + (m + 1) * tile, :] = acc[r, :].astype(jnp.bfloat16)

    def add_piece(s):
        ks = pl.ds(pl.multiple_of(s * k_in, k_in), k_in)
        for m in range(2):
            r = slice(m * tile, (m + 1) * tile)
            acc[r, :] += jnp.dot(
                normed[r, ks], w_in[1, ks, :], preferred_element_type=jnp.float32
            )

    def add_plane(src):
        def body(k, carry):
            add_piece(src * 4 + k)
            return carry

        lax.fori_loop(0, 4, body, 0)

    def pool(flags):
        def body(i, carry):
            base = pl.multiple_of(i * chunk, chunk)
            ext = pl.ds(base, chunk + 16)
            d = docs[ext, :]
            same = []
            count = jnp.ones_like(d)
            for j in range(4):
                ok = jnp.where(pltpu.roll(d, 2**j, 0) == d, flags[j], 0.0)
                same.append(ok)
                count = count + ok * pltpu.roll(count, 2**j, 0)
            for q in range(width // 128):
                cols = slice(q * 128, (q + 1) * 128)
                p = proj[ext, cols].astype(jnp.float32)
                total_sum = p
                for j in range(4):
                    total_sum = total_sum + same[j] * pltpu.roll(total_sum, 2**j, 0)
                v = total_sum / count - p
                pooled[c, pl.ds(base, chunk), cols] = v[16:, :].astype(jnp.bfloat16)
            return carry

        lax.fori_loop(0, total // chunk, body, 0)

    flags = [jnp.where(g >= j, jnp.float32(1.0), jnp.float32(0.0)) for j in range(4)]

    def swap_pooled(l):
        here = pooled.at[c]
        return remote(here, here, pool_sem.at[l, 0], pool_sem.at[l, 1], partner)

    def pooled_arrived(l):
        there = pooled.at[1 - c]
        remote(there, there, pool_sem.at[l, 1], pool_sem.at[l, 1], partner).wait_recv()

    def mix(l, store):
        for m in range(2):
            r = slice(m * tile, (m + 1) * tile)
            y = jnp.dot(pooled[0, r, :], w_mix[l, 0:width, :], preferred_element_type=jnp.float32)
            y = y + jnp.dot(
                pooled[1, r, :], w_mix[l, width : 2 * width, :], preferred_element_type=jnp.float32
            )
            store(r, (y * scale[l : l + 1, :]).astype(jnp.bfloat16))

    def normalize_block(k):
        start = pl.multiple_of(HALO + peer_of(g, k) * own, 16)
        normalize_rows(0, load_tokens, start, own)

    pump_plane("in", 0)

    @pl.when((z > 0) & (g == 3))
    def _():
        remote(halo_here, halo_here, halo.at[0], halo.at[0], partner).wait_recv()
        halo_part.start()
        for k in (1, 2, 3):
            halo_peer[k].start()

    pump_far("in", 0, 1)
    tok_here.wait()
    from_partner(tok_block, tok_prx, 0)
    normalize_block(0)
    for far in range(2, nz - 1):
        pump_far("in", 0, far)
    spread(tok_block, tok_rx, tok_tx, tok_prx, tok_ptx, tok_sent)
    start_weights("mix", 0)
    start_weights("in", 1)
    start_weights("mix", 1)

    @pl.when((z > 0) & (g != 3))
    def _():
        remote(halo_here, halo_here, halo.at[0], halo.at[0], partner).wait_recv()
        halo_part.start()

    for k in (1, 2):
        from_partner(tok_block, tok_prx, k)
        normalize_block(k)

    @pl.when(z > 0)
    def _():
        spot = xt.at[1 - c, pl.ds(0, HALO), :]
        remote(spot, spot, halo.at[1], halo.at[1], partner).wait_recv()

    normalize_rows(0, load_tokens, 0, HALO)
    spread_end(tok_block, tok_rx, tok_prx, tok_ptx, tok_sent)
    pump_plane("mix", 0)
    from_partner(tok_block, tok_prx, 3)
    normalize_block(3)
    docs[16 : 16 + total, :] = xt[0, :, half : half + 128].astype(jnp.float32)
    pump_far("in", 0, nz - 1)
    for far in range(1, nz - 1):
        pump_far("mix", 0, far)
    project(0)
    pump_plane("in", 1)
    pool(flags)
    swap_pooled(0).start()
    pump_far("mix", 0, nz - 1)
    pump_plane("mix", 1)
    pooled_arrived(0)
    mine = g + 4 * c

    def store_acts(r, v):
        acts[mine, r, :] = v

    mix(0, store_acts)
    here = acts.at[mine]
    act_sent = [remote(here, here, act_ptx.at[0], act_prx.at[0], partner)]
    for k in (1, 2):
        act_sent.append(remote(here, here, act_tx.at[k], act_rx.at[k], peer(k)))
    for copy in act_sent[1:] + act_sent[:1]:
        copy.start()

    def act_block(side, q):
        return acts.at[q + 4 * side]

    pump_far("in", 1, 1)
    for far in range(2, nz - 1):
        pump_far("in", 1, far, range(2))
    spread(act_block, act_rx, act_tx, act_prx, act_ptx, act_sent)
    for far in range(2, nz - 1):
        pump_far("in", 1, far, range(2, 4))
    spread_end(act_block, act_rx, act_prx, act_ptx, act_sent)
    for k in range(4):
        from_partner(act_block, act_prx, k)
    normalize_rows(1, load_acts, 0, total)
    acc[...] = jnp.zeros_like(acc)
    add_plane(z)
    for far in range(1, nz - 1):
        @pl.when(z >= far)
        def _():
            add_plane(z - far)

        @pl.when(z + far < nz)
        def _():
            add_plane(z + far)

    @pl.when((z == 0) | (z == nz - 1))
    def _():
        def body(k, carry):
            s = (nz - 1 - z) * 4 + peer_of(g, k)
            arrived("in", 1, s)
            add_piece(s)
            return carry

        lax.fori_loop(0, 4, body, 0)

    proj[16 : 16 + total, :] = acc[...].astype(jnp.bfloat16)
    swap_pooled(0).wait_send()
    pool(flags)
    swap_pooled(1).start()
    pump_line("mix", 1)
    pooled_arrived(1)

    def store_last(r, v):
        last[r, :] = v

    mix(1, store_last)
    place = out.at[:, pl.ds(g * width, width)]
    for k in (1, 2, 3):
        remote(
            last.at[rows_of(peer_of(g, k)), :], place, out_tx.at[k], out_rx.at[k], peer(k)
        ).start()
    keep = pltpu.make_async_copy(last.at[rows_of(g), :], place, out_rx.at[0])
    keep.start()

    swap_pooled(1).wait_send()
    for kind in ("in", "mix"):
        for l in range(2):
            for k in (1, 2, 3):
                give_weight(kind, l, k).wait_send()
            for src in range(nz):
                for k in range(4):
                    s = src * 4 + k

                    @pl.when((z >= src) & (z < nz - 1))
                    def _():
                        relay(kind, l, s, True).wait_send()

                    @pl.when((z <= src) & (z > 0))
                    def _():
                        relay(kind, l, s, False).wait_send()

    @pl.when((z < nz - 1) & (g == 3))
    def _():
        halo_up.wait_send()

    @pl.when(z > 0)
    def _():
        halo_part.wait_send()

        @pl.when(g == 3)
        def _():
            for k in (1, 2, 3):
                halo_peer[k].wait_send()

    for copy in tok_sent + act_sent:
        copy.wait_send()
    for k in (1, 2, 3):
        spot = out.at[:, pl.ds(peer_of(g, k) * width, width)]
        remote(
            last.at[rows_of(peer_of(g, k)), :], spot, out_tx.at[k], out_rx.at[k], peer(k)
        ).wait()
    keep.wait()


def fused_shards(tokens, doc_ids, norm_gain, in_proj, mix_proj, out_scale):
    own, local_width = tokens.shape
    width = local_width // 4
    nsp = lax.axis_size("sp")
    nz = nsp // 4
    total = HALO + 4 * own
    tile_docs = jnp.broadcast_to((doc_ids + 1).astype(jnp.bfloat16)[:, None], (own, 128))
    tok = jnp.concatenate([tokens, tile_docs], axis=1)
    block = lax.axis_index("sp") % 4 + 4 * lax.axis_index("tp")
    scale = lax.dynamic_slice_in_dim(out_scale, block * width, width, 1)
    any_spec = pl.BlockSpec(memory_space=pl.ANY)
    vmem_spec = pl.BlockSpec(memory_space=pltpu.VMEM)
    bf16, f32 = jnp.bfloat16, jnp.float32
    dma = pltpu.SemaphoreType.DMA
    scratch = [
        pltpu.VMEM((2, total, local_width + 128), bf16),
        pltpu.VMEM((total, 8 * width), bf16),
        pltpu.VMEM((8, total, width), bf16),
        pltpu.VMEM((2, 8 * width, width), bf16),
        pltpu.VMEM((2, 2 * width, width), bf16),
        pltpu.VMEM((total, width), f32),
        pltpu.VMEM((16 + total, width), bf16),
        pltpu.VMEM((16 + total, 128), f32),
        pltpu.VMEM((2, total, width), bf16),
        pltpu.VMEM((total, width), bf16),
    ]
    scratch += [dma((2, nsp)) for _ in range(6)] + [dma((2, 4)) for _ in range(2)]
    scratch += [dma((5,)) for _ in range(4)] + [dma((2,)), dma((5,))]
    scratch += [dma((5,)) for _ in range(4)] + [dma((2, 2)), dma((4,)), dma((4,))]
    return pl.pallas_call(
        functools.partial(fused_kernel, nz, own),
        out_shape=jax.ShapeDtypeStruct((own, local_width), bf16),
        in_specs=[any_spec, any_spec, any_spec, vmem_spec, vmem_spec],
        out_specs=any_spec,
        scratch_shapes=scratch,
        compiler_params=pltpu.CompilerParams(
            collective_id=0, has_side_effects=True, vmem_limit_bytes=60 * 1024 * 1024
        ),
    )(tok, in_proj, mix_proj, norm_gain, scale)


def solution(mesh):
    placed = (P("sp", "tp"), P("sp"), P(), P(None, "sp", "tp"), P(None, "sp", "tp"), P())
    body = fused_shards if mesh.shape["tp"] == 2 and mesh.shape["sp"] % 4 == 0 and mesh.shape["sp"] > 12 else shards
    return jax.shard_map(
        body, mesh=mesh, in_specs=placed, out_specs=P("sp", "tp"), check_vma=False
    )
```

profile of v0, /device:TPU:0, one launch (start us, length us, event | category | flops | bytes accessed | tf_op | source)
XLA Modules:
  0.0 204.1 jit_solution(15338044301077740674)
XLA Ops:
  0.0 0.0 copy-start
  0.0 0.7 add_convert_fusion
  0.7 0.1 copy-done
  0.8 0.6 constant_dynamic-slice_fusion.scale
  1.4 0.1 broadcast_in_dim.2
  1.5 2.4 %pad_maximum_fusion.tok = bf16[288,2176]{1,0:T(8,128)(2,1)} fusion(bf16[288,128]{1,0:T(8,128)(2,1)S(1)} %broadcast_in_dim.2, bf16[288,2048]{1,0:T(8,128)(2,1)} %param.6), kind=kLoop, calls=%fused_computation | loop fusion | flops 2506752 | bytes 2506752 | tf_op jit(solution)/shard_map/concatenate | solution.py:570
  3.9 197.8 %shard_map.64 = bf16[288,2048]{1,0:T(8,128)(2,1)} custom-call(bf16[288,2176]{1,0:T(8,128)(2,1)} %pad_maximum_fusion.tok, bf16[2,256,2048]{2,1,0:T(8,128)(2,1)} %in_w.1, bf16[2,64,2048]{2,1,0:T(8,128)(2,1)} %mix_w.1, f32[2,4096]{1,0:T(2,128)} %gain.1, f32[2,512]{1,0:T(2,128)} %constant_dynamic-slice_fusion.scale), custom_call_target="tpu_custom_call" | custom-call | tf_op jit(solution)/shard_map/pallas_call | solution.py:592
  201.7 2.4 %copy.8 = bf16[288,2048]{1,0:T(8,128)(2,1)} copy(bf16[288,2048]{1,0:T(8,128)(2,1)} %shard_map.64) | data formatting | bytes 2359296
Async XLA Ops:
  0.0 0.8 copy-start
where the time goes:
time: 204 us
  Pallas kernels  198 us (97%)
  local copies, waits for them, and re-layouts  3.18 us (2%)
  other arithmetic  3.11 us (2%)
    pallas_call x1, Pallas kernels, fused_shards(): pl.pallas_call(functools.partial(fused_kernel, nz, own), out_shape=jax.Sh...  198 us

commit v1 on v0

--- a/solution.py
+++ b/solution.py
@@ -108,27 +108,46 @@
     return current
 
 
-def peer_of(g, k):
-    return (g // 2 + k // 2) % 2 * 2 + (g % 2 + k % 2) % 2
+SEG = 2
+
+
+def peer_of(p, k):
+    return (p // 2 + k // 2) % 2 * 2 + (p % 2 + k % 2) % 2
+
+
+def place_of(sp):
+    return sp % 2, sp // 2 % 2, sp // 4
 
 
 def fused_kernel(
-    nz, own, tok, in_w, mix_w, gain, scale, out,
+    own, tok, in_w, mix_w, gain, scale, out,
     xt, normed, acts, w_in, w_mix, acc, proj, docs, pooled, last,
-    rx_in, rx_mix, up_in, up_mix, dn_in, dn_mix, tx_in, tx_mix,
+    rx_in, rx_mix, y_in, y_mix, z_in, z_mix, tx_in, tx_mix,
     tok_rx, tok_prx, tok_tx, tok_ptx, halo, halo_tx, act_rx, act_prx, act_tx, act_ptx,
     pool_sem, out_rx, out_tx,
 ):
     sp = lax.axis_index("sp")
     c = lax.axis_index("tp")
-    z, g = sp // 4, sp % 4
-    total = HALO + 4 * own
+    nsp = lax.axis_size("sp")
+    x, y, z = place_of(sp)
+    half_z, g = z // 2, x + 2 * (z % 2)
+    seg = HALO + 2 * own
+    total = SEG * seg
     width = w_in.shape[2]
     k_in, k_mix = in_w.shape[1], mix_w.shape[1]
     partner = (sp, 1 - c)
 
+    def sp_at(p, row, upper):
+        return 4 * (2 * upper + p // 2) + 2 * row + p % 2
+
     def peer(k):
-        return (z * 4 + peer_of(g, k), c)
+        return (sp_at(peer_of(g, k), y, half_z), c)
+
+    beside = (sp_at(g, 1 - y, half_z), c)
+    across = (sp_at(g, y, 1 - half_z), c)
+    behind = [4 * (2 * half_z + i) + 2 * y - 1 for i in range(SEG)]
+    next_x, next_y, next_z = place_of(sp + 1)
+    feeds = (x == 1) & (sp + 1 < nsp)
 
     def remote(src, dst, tx, rx, to):
         return pltpu.make_async_remote_copy(
@@ -143,18 +162,20 @@
 
     for k in (1, 2, 3):
         greet(peer(k))
-    greet(partner)
-
-    @pl.when(z > 0)
+    for to in (partner, beside, across):
+        greet(to)
+    for i in range(SEG):
+        @pl.when(behind[i] >= 0)
+        def _():
+            greet((behind[i], c))
+
+    @pl.when(feeds)
     def _():
-        greet((sp - 4, c))
-
-    @pl.when(z < nz - 1)
-    def _():
-        greet((sp + 4, c))
-
-    ends = jnp.where(z > 0, 1, 0) + jnp.where(z < nz - 1, 1, 0)
-    pl.semaphore_wait(barrier, 4 + ends)
+        for p in range(4):
+            greet((sp_at(p, next_y, next_z // 2), c))
+
+    fed = [jnp.where(behind[i] >= 0, 1, 0) for i in range(SEG)]
+    pl.semaphore_wait(barrier, 6 + fed[0] + fed[1] + jnp.where(feeds, 4, 0))
 
     def in_piece(l, s):
         return w_in.at[l, pl.ds(s * k_in, k_in), :]
@@ -163,8 +184,8 @@
         return w_mix.at[l, pl.ds(s * k_mix, k_mix), :]
 
     kinds = {
-        "in": (in_piece, in_w, rx_in, up_in, dn_in, tx_in),
-        "mix": (mix_piece, mix_w, rx_mix, up_mix, dn_mix, tx_mix),
+        "in": (in_piece, in_w, rx_in, y_in, z_in, tx_in),
+        "mix": (mix_piece, mix_w, rx_mix, y_mix, z_mix, tx_mix),
     }
 
     def own_weight(kind, l):
@@ -180,66 +201,64 @@
             tx.at[l, k], rx.at[l, sp], peer(k),
         )
 
-    def relay(kind, l, s, up):
-        piece, _, rx, up_tx, dn_tx, _ = kinds[kind]
-        tx = up_tx if up else dn_tx
-        to = sp + 4 if up else sp - 4
-        return remote(piece(l, s), piece(l, s), tx.at[l, s], rx.at[l, s], (to, c))
+    def to_beside(kind, l, s):
+        piece, _, rx, tx = kinds[kind][:4]
+        return remote(piece(l, s), piece(l, s), tx.at[l, s], rx.at[l, s], beside)
+
+    def to_across(kind, l, s):
+        piece, _, rx, _, tx = kinds[kind][:5]
+        return remote(piece(l, s), piece(l, s), tx.at[l, s], rx.at[l, s], across)
 
     def arrived(kind, l, s):
         piece, _, rx = kinds[kind][:3]
         remote(piece(l, s), piece(l, s), rx.at[l, s], rx.at[l, s], partner).wait_recv()
 
-    def send_relay(kind, l, s, up):
-        @pl.when((z < nz - 1) if up else (z > 0))
-        def _():
-            relay(kind, l, s, up).start()
-
-    def pump_plane(kind, l):
-        own_weight(kind, l).wait()
-        send_relay(kind, l, sp, True)
-        send_relay(kind, l, sp, False)
-        for k in (1, 2, 3):
-            s = z * 4 + peer_of(g, k)
-            arrived(kind, l, s)
-            send_relay(kind, l, s, True)
-            send_relay(kind, l, s, False)
-
-    def pump_far(kind, l, far, ks=range(4)):
+    def home(k):
+        return sp_at(peer_of(g, k), y, half_z)
+
+    def away(k):
+        return sp_at(peer_of(g, k), y, 1 - half_z)
+
+    def pump_home(kind, l, ks=range(4)):
         for k in ks:
-            @pl.when(z >= far)
-            def _():
-                s = (z - far) * 4 + peer_of(g, k)
-                arrived(kind, l, s)
-                send_relay(kind, l, s, True)
-
-            @pl.when(z + far < nz)
-            def _():
-                s = (z + far) * 4 + peer_of(g, k)
-                arrived(kind, l, s)
-                send_relay(kind, l, s, False)
-
-    def pump_line(kind, l):
-        for far in range(1, nz):
-            pump_far(kind, l, far)
+            if k == 0:
+                own_weight(kind, l).wait()
+            else:
+                arrived(kind, l, home(k))
+            to_across(kind, l, home(k)).start()
+            to_beside(kind, l, home(k)).start()
+
+    def pump_away(kind, l, ks=range(4)):
+        for k in ks:
+            arrived(kind, l, away(k))
+            to_beside(kind, l, away(k)).start()
+
+    def from_beside(kind, l):
+        for k in range(4):
+            arrived(kind, l, sp_at(peer_of(g, k), 1 - y, half_z))
+            arrived(kind, l, sp_at(peer_of(g, k), 1 - y, 1 - half_z))
 
     def start_weights(kind, l):
         own_weight(kind, l).start()
         for k in (1, 2, 3):
             give_weight(kind, l, k).start()
 
+    def row_of(q):
+        return q // 2 * seg + HALO + q % 2 * own
+
     def rows_of(q):
-        return pl.ds(HALO + q * own, own)
-
-    halo_here = xt.at[c, pl.ds(0, HALO), :]
-    tail = tok.at[pl.ds(own - HALO, HALO), :]
-    halo_up = remote(tail, halo_here, halo_tx.at[0], halo.at[0], (sp + 4, c))
-    halo_peer = {k: remote(halo_here, halo_here, halo_tx.at[k], halo.at[0], peer(k)) for k in (1, 2, 3)}
-    halo_part = remote(halo_here, halo_here, halo_tx.at[4], halo.at[1], partner)
-
-    @pl.when((z < nz - 1) & (g == 3))
-    def _():
-        halo_up.start()
+        return pl.ds(pl.multiple_of(row_of(q), 16), own)
+
+    def halo_at(side, i):
+        return xt.at[side, pl.ds(pl.multiple_of(i * seg, 16), HALO), :]
+
+    def halo_send(p):
+        to = (sp_at(p, next_y, next_z // 2), c)
+        tail = tok.at[pl.ds(own - HALO, HALO), :]
+        return remote(tail, halo_at(c, next_z % 2), halo_tx.at[p], halo.at[next_z % 2], to)
+
+    def halo_part(i):
+        return remote(halo_at(c, i), halo_at(c, i), halo_tx.at[4 + i], halo.at[2 + i], partner)
 
     start_weights("in", 0)
     tok_here = pltpu.make_async_copy(tok, xt.at[c, rows_of(g), :], tok_rx.at[0])
@@ -252,7 +271,12 @@
     for copy in tok_sent:
         copy.start()
 
-    @pl.when(z == 0)
+    @pl.when(feeds)
+    def _():
+        for p in range(4):
+            halo_send(p).start()
+
+    @pl.when(behind[0] < 0)
     def _():
         xt[:, 0:HALO, :] = jnp.zeros((2, HALO, xt.shape[2]), xt.dtype)
 
@@ -260,25 +284,20 @@
     proj[0:16, :] = jnp.zeros((16, width), proj.dtype)
 
     def spread(block, rx, tx, prx, ptx, sent):
-        for k in (1, 2):
+        for k in (2, 1):
             spot = block(c, peer_of(g, k))
             remote(spot, spot, rx.at[k], rx.at[k], partner).wait_recv()
-        for k in (1, 2):
-            part = half_of(block(c, peer_of(g, k)), k)
-            copy = remote(part, part, tx.at[2 + k], rx.at[2 + k], peer(3 - k))
-            copy.start()
-            sent.append(copy)
-        for k in (1, 2):
-            spot = block(c, peer_of(g, k))
+            if k == 2:
+                copy = remote(spot, spot, tx.at[3], rx.at[3], peer(1))
+                copy.start()
+                sent.append(copy)
             copy = remote(spot, spot, ptx.at[k], prx.at[k], partner)
             copy.start()
             sent.append(copy)
 
     def spread_end(block, rx, prx, ptx, sent):
         spot = block(c, peer_of(g, 3))
-        for k in (1, 2):
-            part = half_of(spot, k)
-            remote(part, part, rx.at[2 + k], rx.at[2 + k], partner).wait_recv()
+        remote(spot, spot, rx.at[3], rx.at[3], partner).wait_recv()
         copy = remote(spot, spot, ptx.at[3], prx.at[3], partner)
         copy.start()
         sent.append(copy)
@@ -286,10 +305,6 @@
     def from_partner(block, prx, k):
         spot = block(1 - c, peer_of(g, k))
         remote(spot, spot, prx.at[k], prx.at[k], partner).wait_recv()
-
-    def half_of(spot, k):
-        n = spot.shape[0] // 2
-        return spot.at[pl.ds((k - 1) * n, n), :]
 
     def tok_block(side, q):
         return xt.at[side, rows_of(q), :]
@@ -344,6 +359,7 @@
             proj[16 + m * tile : 16 + (m + 1) * tile, :] = acc[r, :].astype(jnp.bfloat16)
 
     def add_piece(s):
+        s = jnp.int32(s)
         ks = pl.ds(pl.multiple_of(s * k_in, k_in), k_in)
         for m in range(2):
             r = slice(m * tile, (m + 1) * tile)
@@ -351,9 +367,9 @@
                 normed[r, ks], w_in[1, ks, :], preferred_element_type=jnp.float32
             )
 
-    def add_plane(src):
+    def add_group(row, upper):
         def body(k, carry):
-            add_piece(src * 4 + k)
+            add_piece(sp_at(k, row, upper))
             return carry
 
         lax.fori_loop(0, 4, body, 0)
@@ -401,58 +417,50 @@
             store(r, (y * scale[l : l + 1, :]).astype(jnp.bfloat16))
 
     def normalize_block(k):
-        start = pl.multiple_of(HALO + peer_of(g, k) * own, 16)
+        start = pl.multiple_of(row_of(peer_of(g, k)), 16)
         normalize_rows(0, load_tokens, start, own)
 
-    pump_plane("in", 0)
-
-    @pl.when((z > 0) & (g == 3))
-    def _():
-        remote(halo_here, halo_here, halo.at[0], halo.at[0], partner).wait_recv()
-        halo_part.start()
-        for k in (1, 2, 3):
-            halo_peer[k].start()
-
-    pump_far("in", 0, 1)
+    pump_home("in", 0)
     tok_here.wait()
-    from_partner(tok_block, tok_prx, 0)
-    normalize_block(0)
-    for far in range(2, nz - 1):
-        pump_far("in", 0, far)
     spread(tok_block, tok_rx, tok_tx, tok_prx, tok_ptx, tok_sent)
     start_weights("mix", 0)
     start_weights("in", 1)
     start_weights("mix", 1)
-
-    @pl.when((z > 0) & (g != 3))
-    def _():
-        remote(halo_here, halo_here, halo.at[0], halo.at[0], partner).wait_recv()
-        halo_part.start()
-
-    for k in (1, 2):
+    pump_away("in", 0)
+
+    for i in range(SEG):
+        @pl.when(behind[i] >= 0)
+        def _():
+            spot = halo_at(c, i)
+            remote(spot, spot, halo.at[i], halo.at[i], partner).wait_recv()
+            halo_part(i).start()
+
+    from_partner(tok_block, tok_prx, 0)
+    normalize_block(0)
+    pump_home("mix", 0)
+    for k in (2, 1):
         from_partner(tok_block, tok_prx, k)
         normalize_block(k)
-
-    @pl.when(z > 0)
-    def _():
-        spot = xt.at[1 - c, pl.ds(0, HALO), :]
-        remote(spot, spot, halo.at[1], halo.at[1], partner).wait_recv()
-
-    normalize_rows(0, load_tokens, 0, HALO)
+    pump_away("mix", 0)
     spread_end(tok_block, tok_rx, tok_prx, tok_ptx, tok_sent)
-    pump_plane("mix", 0)
+    pump_home("in", 1)
+    for i in range(SEG):
+        @pl.when(behind[i] >= 0)
+        def _():
+            spot = halo_at(1 - c, i)
+            remote(spot, spot, halo.at[2 + i], halo.at[2 + i], partner).wait_recv()
+
+        normalize_rows(0, load_tokens, i * seg, HALO)
+    pump_home("mix", 1)
     from_partner(tok_block, tok_prx, 3)
     normalize_block(3)
     docs[16 : 16 + total, :] = xt[0, :, half : half + 128].astype(jnp.float32)
-    pump_far("in", 0, nz - 1)
-    for far in range(1, nz - 1):
-        pump_far("mix", 0, far)
+    from_beside("in", 0)
     project(0)
-    pump_plane("in", 1)
     pool(flags)
     swap_pooled(0).start()
-    pump_far("mix", 0, nz - 1)
-    pump_plane("mix", 1)
+    from_beside("mix", 0)
+    pump_away("in", 1)
     pooled_arrived(0)
     mine = g + 4 * c
 
@@ -470,42 +478,23 @@
     def act_block(side, q):
         return acts.at[q + 4 * side]
 
-    pump_far("in", 1, 1)
-    for far in range(2, nz - 1):
-        pump_far("in", 1, far, range(2))
+    pump_away("mix", 1)
     spread(act_block, act_rx, act_tx, act_prx, act_ptx, act_sent)
-    for far in range(2, nz - 1):
-        pump_far("in", 1, far, range(2, 4))
     spread_end(act_block, act_rx, act_prx, act_ptx, act_sent)
     for k in range(4):
         from_partner(act_block, act_prx, k)
     normalize_rows(1, load_acts, 0, total)
     acc[...] = jnp.zeros_like(acc)
-    add_plane(z)
-    for far in range(1, nz - 1):
-        @pl.when(z >= far)
-        def _():
-            add_plane(z - far)
-
-        @pl.when(z + far < nz)
-        def _():
-            add_plane(z + far)
-
-    @pl.when((z == 0) | (z == nz - 1))
-    def _():
-        def body(k, carry):
-            s = (nz - 1 - z) * 4 + peer_of(g, k)
-            arrived("in", 1, s)
-            add_piece(s)
-            return carry
-
-        lax.fori_loop(0, 4, body, 0)
-
+    add_group(y, half_z)
+    add_group(y, 1 - half_z)
+    from_beside("in", 1)
+    add_group(1 - y, half_z)
+    add_group(1 - y, 1 - half_z)
     proj[16 : 16 + total, :] = acc[...].astype(jnp.bfloat16)
     swap_pooled(0).wait_send()
     pool(flags)
     swap_pooled(1).start()
-    pump_line("mix", 1)
+    from_beside("mix", 1)
     pooled_arrived(1)
 
     def store_last(r, v):
@@ -525,30 +514,20 @@
         for l in range(2):
             for k in (1, 2, 3):
                 give_weight(kind, l, k).wait_send()
-            for src in range(nz):
-                for k in range(4):
-                    s = src * 4 + k
-
-                    @pl.when((z >= src) & (z < nz - 1))
-                    def _():
-                        relay(kind, l, s, True).wait_send()
-
-                    @pl.when((z <= src) & (z > 0))
-                    def _():
-                        relay(kind, l, s, False).wait_send()
-
-    @pl.when((z < nz - 1) & (g == 3))
+            for k in range(4):
+                to_across(kind, l, home(k)).wait_send()
+                to_beside(kind, l, home(k)).wait_send()
+                to_beside(kind, l, away(k)).wait_send()
+
+    @pl.when(feeds)
     def _():
-        halo_up.wait_send()
-
-    @pl.when(z > 0)
-    def _():
-        halo_part.wait_send()
-
-        @pl.when(g == 3)
+        for p in range(4):
+            halo_send(p).wait_send()
+
+    for i in range(SEG):
+        @pl.when(behind[i] >= 0)
         def _():
-            for k in (1, 2, 3):
-                halo_peer[k].wait_send()
+            halo_part(i).wait_send()
 
     for copy in tok_sent + act_sent:
         copy.wait_send()
@@ -564,11 +543,11 @@
     own, local_width = tokens.shape
     width = local_width // 4
     nsp = lax.axis_size("sp")
-    nz = nsp // 4
-    total = HALO + 4 * own
+    total = SEG * (HALO + 2 * own)
     tile_docs = jnp.broadcast_to((doc_ids + 1).astype(jnp.bfloat16)[:, None], (own, 128))
     tok = jnp.concatenate([tokens, tile_docs], axis=1)
-    block = lax.axis_index("sp") % 4 + 4 * lax.axis_index("tp")
+    x, _, z = place_of(lax.axis_index("sp"))
+    block = x + 2 * (z % 2) + 4 * lax.axis_index("tp")
     scale = lax.dynamic_slice_in_dim(out_scale, block * width, width, 1)
     any_spec = pl.BlockSpec(memory_space=pl.ANY)
     vmem_spec = pl.BlockSpec(memory_space=pltpu.VMEM)
@@ -587,10 +566,10 @@
         pltpu.VMEM((total, width), bf16),
     ]
     scratch += [dma((2, nsp)) for _ in range(6)] + [dma((2, 4)) for _ in range(2)]
-    scratch += [dma((5,)) for _ in range(4)] + [dma((2,)), dma((5,))]
+    scratch += [dma((5,)) for _ in range(4)] + [dma((4,)), dma((6,))]
     scratch += [dma((5,)) for _ in range(4)] + [dma((2, 2)), dma((4,)), dma((4,))]
     return pl.pallas_call(
-        functools.partial(fused_kernel, nz, own),
+        functools.partial(fused_kernel, own),
         out_shape=jax.ShapeDtypeStruct((own, local_width), bf16),
         in_specs=[any_spec, any_spec, any_spec, vmem_spec, vmem_spec],
         out_specs=any_spec,
@@ -603,7 +582,7 @@
 
 def solution(mesh):
     placed = (P("sp", "tp"), P("sp"), P(), P(None, "sp", "tp"), P(None, "sp", "tp"), P())
-    body = fused_shards if mesh.shape["tp"] == 2 and mesh.shape["sp"] % 4 == 0 and mesh.shape["sp"] > 12 else shards
+    body = fused_shards if mesh.shape["tp"] == 2 and mesh.shape["sp"] == 16 else shards
     return jax.shard_map(
         body, mesh=mesh, in_specs=placed, out_specs=P("sp", "tp"), check_vma=False
     )

time: 204 us -> 272 us (1.33)
  Pallas kernels: 198 us -> 266 us
    pallas_call x1, Pallas kernels: 198 us -> 266 us  [fused_shards(): pl.pallas_call(functools.partial(fused_kernel, own), out_shape=jax.ShapeD...]
where the time goes in v1:
time: 272 us
  Pallas kernels  266 us (98%)
  local copies, waits for them, and re-layouts  3.18 us (1%)
  other arithmetic  3.11 us (1%)
    pallas_call x1, Pallas kernels, fused_shards(): pl.pallas_call(functools.partial(fused_kernel, own), out_shape=jax.ShapeD...  266 us

profile of v1, /device:TPU:0, one launch (start us, length us, event | category | flops | bytes accessed | tf_op | source)
XLA Modules:
  0.0 272.0 jit_solution(16032809741657618470)
XLA Ops:
  0.0 0.0 copy-start
  0.0 0.7 add_convert_fusion
  0.7 0.1 copy-done
  0.8 0.6 constant_dynamic-slice_fusion.scale
  1.4 0.1 broadcast_in_dim.2
  1.5 2.4 pad_maximum_fusion.tok
  3.9 265.7 %shard_map.64 = bf16[288,2048]{1,0:T(8,128)(2,1)} custom-call(bf16[288,2176]{1,0:T(8,128)(2,1)} %pad_maximum_fusion.tok, bf16[2,256,2048]{2,1,0:T(8,128)(2,1)} %in_w.1, bf16[2,64,2048]{2,1,0:T(8,128)(2,1)} %mix_w.1, f32[2,4096]{1,0:T(2,128)} %gain.1, f32[2,512]{1,0:T(2,128)} %constant_dynamic-slice_fusion.scale), custom_call_target="tpu_custom_call" | custom-call | tf_op jit(solution)/shard_map/pallas_call | solution.py:571
  269.6 2.4 copy.8
Async XLA Ops:
  0.0 0.8 copy-start

commit v2 on v0

--- a/solution.py
+++ b/solution.py
@@ -108,6 +108,9 @@
     return current
 
 
+PARTS = ((0, 0, 4), (1, 0, 2), (1, 2, 1), (1, 3, 1))
+
+
 def peer_of(g, k):
     return (g // 2 + k // 2) % 2 * 2 + (g % 2 + k % 2) % 2
 
@@ -159,46 +162,57 @@
     def in_piece(l, s):
         return w_in.at[l, pl.ds(s * k_in, k_in), :]
 
+    def columns(kind, l, block):
+        if kind == "in":
+            return l, pl.ds(block * width, width)
+        layer, first, count = PARTS[l]
+        unit = width // 4
+        return layer, pl.ds(block * width + first * unit, count * unit)
+
     def mix_piece(l, s):
-        return w_mix.at[l, pl.ds(s * k_mix, k_mix), :]
+        layer, cols = columns("mix", l, 0)
+        return w_mix.at[layer, pl.ds(s * k_mix, k_mix), cols]
 
     kinds = {
         "in": (in_piece, in_w, rx_in, up_in, dn_in, tx_in),
         "mix": (mix_piece, mix_w, rx_mix, up_mix, dn_mix, tx_mix),
     }
 
+    def given(kind, l, block):
+        layer, cols = columns(kind, l, block)
+        return kinds[kind][1].at[layer, :, cols]
+
     def own_weight(kind, l):
-        piece, src, rx = kinds[kind][:3]
-        return pltpu.make_async_copy(
-            src.at[l, :, pl.ds(g * width, width)], piece(l, sp), rx.at[l, sp]
+        piece, _, rx = kinds[kind][:3]
+        return pltpu.make_async_copy(given(kind, l, g), piece(l, sp), rx.at[l, sp])
+
+    def give_weight(kind, l, k):
+        piece, _, rx, _, _, tx = kinds[kind]
+        return remote(
+            given(kind, l, peer_of(g, k)), piece(l, sp), tx.at[l, k], rx.at[l, sp], peer(k),
         )
 
-    def give_weight(kind, l, k):
-        piece, src, rx, _, _, tx = kinds[kind]
-        return remote(
-            src.at[l, :, pl.ds(peer_of(g, k) * width, width)], piece(l, sp),
-            tx.at[l, k], rx.at[l, sp], peer(k),
-        )
-
-    def relay(kind, l, s, up):
+    def relay(kind, l, s, up, src=None):
         piece, _, rx, up_tx, dn_tx, _ = kinds[kind]
         tx = up_tx if up else dn_tx
         to = sp + 4 if up else sp - 4
-        return remote(piece(l, s), piece(l, s), tx.at[l, s], rx.at[l, s], (to, c))
+        src = piece(l, s) if src is None else src
+        return remote(src, piece(l, s), tx.at[l, s], rx.at[l, s], (to, c))
 
     def arrived(kind, l, s):
         piece, _, rx = kinds[kind][:3]
         remote(piece(l, s), piece(l, s), rx.at[l, s], rx.at[l, s], partner).wait_recv()
 
-    def send_relay(kind, l, s, up):
+    def send_relay(kind, l, s, up, src=None):
         @pl.when((z < nz - 1) if up else (z > 0))
         def _():
-            relay(kind, l, s, up).start()
+            relay(kind, l, s, up, src).start()
 
     def pump_plane(kind, l):
-        own_weight(kind, l).wait()
-        send_relay(kind, l, sp, True)
-        send_relay(kind, l, sp, False)
+        if kind == "mix" or l:
+            own_weight(kind, l).wait()
+            send_relay(kind, l, sp, True)
+            send_relay(kind, l, sp, False)
         for k in (1, 2, 3):
             s = z * 4 + peer_of(g, k)
             arrived(kind, l, s)
@@ -241,6 +255,8 @@
     def _():
         halo_up.start()
 
+    for up in (True, False):
+        send_relay("in", 0, sp, up, given("in", 0, g))
     start_weights("in", 0)
     tok_here = pltpu.make_async_copy(tok, xt.at[c, rows_of(g), :], tok_rx.at[0])
     tok_here.start()
@@ -391,14 +407,18 @@
         there = pooled.at[1 - c]
         remote(there, there, pool_sem.at[l, 1], pool_sem.at[l, 1], partner).wait_recv()
 
-    def mix(l, store):
+    def mix(part, store):
+        l, cols = columns("mix", part, 0)
         for m in range(2):
             r = slice(m * tile, (m + 1) * tile)
-            y = jnp.dot(pooled[0, r, :], w_mix[l, 0:width, :], preferred_element_type=jnp.float32)
+            y = jnp.dot(
+                pooled[0, r, :], w_mix[l, 0:width, cols], preferred_element_type=jnp.float32
+            )
             y = y + jnp.dot(
-                pooled[1, r, :], w_mix[l, width : 2 * width, :], preferred_element_type=jnp.float32
+                pooled[1, r, :], w_mix[l, width : 2 * width, cols],
+                preferred_element_type=jnp.float32,
             )
-            store(r, (y * scale[l : l + 1, :]).astype(jnp.bfloat16))
+            store(r, cols, (y * scale[l : l + 1, cols]).astype(jnp.bfloat16))
 
     def normalize_block(k):
         start = pl.multiple_of(HALO + peer_of(g, k) * own, 16)
@@ -422,7 +442,8 @@
     spread(tok_block, tok_rx, tok_tx, tok_prx, tok_ptx, tok_sent)
     start_weights("mix", 0)
     start_weights("in", 1)
-    start_weights("mix", 1)
+    for part in (1, 2, 3):
+        start_weights("mix", part)
 
     @pl.when((z > 0) & (g != 3))
     def _():
@@ -447,17 +468,19 @@
     pump_far("in", 0, nz - 1)
     for far in range(1, nz - 1):
         pump_far("mix", 0, far)
+    own_weight("in", 0).wait()
     project(0)
     pump_plane("in", 1)
     pool(flags)
     swap_pooled(0).start()
     pump_far("mix", 0, nz - 1)
-    pump_plane("mix", 1)
+    for part in (1, 2, 3):
+        pump_plane("mix", part)
     pooled_arrived(0)
     mine = g + 4 * c
 
-    def store_acts(r, v):
-        acts[mine, r, :] = v
+    def store_acts(r, cols, v):
+        acts[mine, r, cols] = v
 
     mix(0, store_acts)
     here = acts.at[mine]
@@ -505,24 +528,29 @@
     swap_pooled(0).wait_send()
     pool(flags)
     swap_pooled(1).start()
-    pump_line("mix", 1)
-    pooled_arrived(1)
-
-    def store_last(r, v):
-        last[r, :] = v
-
-    mix(1, store_last)
-    place = out.at[:, pl.ds(g * width, width)]
-    for k in (1, 2, 3):
-        remote(
-            last.at[rows_of(peer_of(g, k)), :], place, out_tx.at[k], out_rx.at[k], peer(k)
-        ).start()
-    keep = pltpu.make_async_copy(last.at[rows_of(g), :], place, out_rx.at[0])
-    keep.start()
+    def store_last(r, cols, v):
+        last[r, cols] = v
+
+    def out_copy(part, k):
+        _, place = columns("mix", part, g)
+        _, cols = columns("mix", part, 0)
+        src = last.at[rows_of(peer_of(g, k)), cols]
+        dst = out.at[:, place]
+        if k == 0:
+            return pltpu.make_async_copy(src, dst, out_rx.at[part, 0])
+        return remote(src, dst, out_tx.at[part, k], out_rx.at[part, k], peer(k))
+
+    for part in (1, 2, 3):
+        pump_line("mix", part)
+        if part == 1:
+            pooled_arrived(1)
+        mix(part, store_last)
+        for k in (1, 2, 3, 0):
+            out_copy(part, k).start()
 
     swap_pooled(1).wait_send()
     for kind in ("in", "mix"):
-        for l in range(2):
+        for l in range(2 if kind == "in" else len(PARTS)):
             for k in (1, 2, 3):
                 give_weight(kind, l, k).wait_send()
             for src in range(nz):
@@ -552,12 +580,15 @@
 
     for copy in tok_sent + act_sent:
         copy.wait_send()
-    for k in (1, 2, 3):
-        spot = out.at[:, pl.ds(peer_of(g, k) * width, width)]
-        remote(
-            last.at[rows_of(peer_of(g, k)), :], spot, out_tx.at[k], out_rx.at[k], peer(k)
-        ).wait()
-    keep.wait()
+    for part in (1, 2, 3):
+        for k in (1, 2, 3):
+            _, place = columns("mix", part, peer_of(g, k))
+            _, cols = columns("mix", part, 0)
+            remote(
+                last.at[rows_of(peer_of(g, k)), cols], out.at[:, place],
+                out_tx.at[part, k], out_rx.at[part, k], peer(k),
+            ).wait()
+        out_copy(part, 0).wait()
 
 
 def fused_shards(tokens, doc_ids, norm_gain, in_proj, mix_proj, out_scale):
@@ -586,9 +617,11 @@
         pltpu.VMEM((2, total, width), bf16),
         pltpu.VMEM((total, width), bf16),
     ]
-    scratch += [dma((2, nsp)) for _ in range(6)] + [dma((2, 4)) for _ in range(2)]
+    parts = len(PARTS)
+    scratch += [dma((n, nsp)) for _ in range(3) for n in (2, parts)]
+    scratch += [dma((2, 4)), dma((parts, 4))]
     scratch += [dma((5,)) for _ in range(4)] + [dma((2,)), dma((5,))]
-    scratch += [dma((5,)) for _ in range(4)] + [dma((2, 2)), dma((4,)), dma((4,))]
+    scratch += [dma((5,)) for _ in range(4)] + [dma((2, 2)), dma((parts, 4)), dma((parts, 4))]
     return pl.pallas_call(
         functools.partial(fused_kernel, nz, own),
         out_shape=jax.ShapeDtypeStruct((own, local_width), bf16),
@@ -603,7 +636,7 @@
 
 def solution(mesh):
     placed = (P("sp", "tp"), P("sp"), P(), P(None, "sp", "tp"), P(None, "sp", "tp"), P())
-    body = fused_shards if mesh.shape["tp"] == 2 and mesh.shape["sp"] % 4 == 0 and mesh.shape["sp"] > 12 else shards
+    body = fused_shards if mesh.shape["tp"] == 2 and mesh.shape["sp"] == 16 else shards
     return jax.shard_map(
         body, mesh=mesh, in_specs=placed, out_specs=P("sp", "tp"), check_vma=False
     )

time: 204 us -> 203 us (level)
  no operation moved by 1% of the time
where the time goes in v2:
time: 203 us
  Pallas kernels  196 us (97%)
  local copies, waits for them, and re-layouts  3.18 us (2%)
  other arithmetic  3.11 us (2%)
    pallas_call x1, Pallas kernels, fused_shards(): pl.pallas_call(functools.partial(fused_kernel, nz, own), out_shape=jax.Sh...  196 us

profile of v2, /device:TPU:0, one launch (start us, length us, event | category | flops | bytes accessed | tf_op | source)
XLA Modules:
  0.0 202.7 jit_solution(15405042370499211672)
XLA Ops:
  0.0 0.0 copy-start
  0.0 0.7 add_convert_fusion
  0.7 0.1 copy-done
  0.8 0.6 constant_dynamic-slice_fusion.scale
  1.4 0.1 broadcast_in_dim.2
  1.5 2.4 %pad_maximum_fusion.tok = bf16[288,2176]{1,0:T(8,128)(2,1)} fusion(bf16[288,128]{1,0:T(8,128)(2,1)S(1)} %broadcast_in_dim.2, bf16[288,2048]{1,0:T(8,128)(2,1)} %param.6), kind=kLoop, calls=%fused_computation | loop fusion | flops 2506752 | bytes 2506752 | tf_op jit(solution)/shard_map/concatenate | solution.py:601
  3.9 196.4 %shard_map.64 = bf16[288,2048]{1,0:T(8,128)(2,1)} custom-call(bf16[288,2176]{1,0:T(8,128)(2,1)} %pad_maximum_fusion.tok, bf16[2,256,2048]{2,1,0:T(8,128)(2,1)} %in_w.1, bf16[2,64,2048]{2,1,0:T(8,128)(2,1)} %mix_w.1, f32[2,4096]{1,0:T(2,128)} %gain.1, f32[2,512]{1,0:T(2,128)} %constant_dynamic-slice_fusion.scale), custom_call_target="tpu_custom_call" | custom-call | tf_op jit(solution)/shard_map/pallas_call | solution.py:625
  200.3 2.4 %copy.8 = bf16[288,2048]{1,0:T(8,128)(2,1)} copy(bf16[288,2048]{1,0:T(8,128)(2,1)} %shard_map.64) | data formatting | bytes 2359296
Async XLA Ops:
  0.0 0.8 copy-start

commit v3 on v2

--- a/solution.py
+++ b/solution.py
@@ -108,7 +108,9 @@
     return current
 
 
-PARTS = ((0, 0, 4), (1, 0, 2), (1, 2, 1), (1, 3, 1))
+PARTS = ((0, 0, 4), (1, 0, 2), (1, 2, 2))
+
+LAST_PARTS = range(1, len(PARTS))
 
 
 def peer_of(g, k):
@@ -116,9 +118,10 @@
 
 
 def fused_kernel(
-    nz, own, tok, in_w, mix_w, gain, scale, out,
+    nz, own, tok, doc_tile, in_w, mix_w, gain, scale, out,
     xt, normed, acts, w_in, w_mix, acc, proj, docs, pooled, last,
-    rx_in, rx_mix, up_in, up_mix, dn_in, dn_mix, tx_in, tx_mix,
+    rx_in, rx_mix, up_in, up_mix, dn_in, dn_mix, tx_in, tx_mix, rx_far,
+    tiles, tile_rx, tile_tx,
     tok_rx, tok_prx, tok_tx, tok_ptx, halo, halo_tx, act_rx, act_prx, act_tx, act_ptx,
     pool_sem, out_rx, out_tx,
 ):
@@ -237,6 +240,40 @@
         for far in range(1, nz):
             pump_far(kind, l, far)
 
+    def plane_piece(part, src):
+        layer, cols = columns("mix", part, 0)
+        return w_mix.at[layer, pl.ds(src * 4 * k_mix, 4 * k_mix), cols]
+
+    def plane_relay(part, src, up):
+        tx = up_mix if up else dn_mix
+        spot, to = plane_piece(part, src), (sp + 4 if up else sp - 4, c)
+        return remote(spot, spot, tx.at[part, src], rx_far.at[part, src], to)
+
+    def send_plane(part, src, up):
+        @pl.when((z < nz - 1) if up else (z > 0))
+        def _():
+            plane_relay(part, src, up).start()
+
+    def pump_own_part(part):
+        own_weight("mix", part).wait()
+        for k in (1, 2, 3):
+            arrived("mix", part, z * 4 + peer_of(g, k))
+        send_plane(part, z, True)
+        send_plane(part, z, False)
+
+    def far_part(part, far, below):
+        src = z - far if below else z + far
+        spot = plane_piece(part, src)
+        remote(spot, spot, rx_far.at[part, src], rx_far.at[part, src], partner).wait_recv()
+        send_plane(part, src, below)
+
+    def far_parts(part):
+        for far in range(1, nz):
+            for below in (True, False):
+                @pl.when((z >= far) if below else (z + far < nz))
+                def _():
+                    far_part(part, far, below)
+
     def start_weights(kind, l):
         own_weight(kind, l).start()
         for k in (1, 2, 3):
@@ -251,9 +288,18 @@
     halo_peer = {k: remote(halo_here, halo_here, halo_tx.at[k], halo.at[0], peer(k)) for k in (1, 2, 3)}
     halo_part = remote(halo_here, halo_here, halo_tx.at[4], halo.at[1], partner)
 
+    own_tile = pltpu.make_async_copy(doc_tile, tiles.at[g], tile_rx.at[g])
+    own_tile.start()
+    tile_sent = [remote(doc_tile, tiles.at[g], tile_tx.at[k], tile_rx.at[g], peer(k)) for k in (1, 2, 3)]
+    tile_up = remote(doc_tile, tiles.at[4], tile_tx.at[0], tile_rx.at[4], (sp + 4, c))
+    tile_on = [remote(tiles.at[4], tiles.at[4], tile_tx.at[3 + k], tile_rx.at[4], peer(k)) for k in (1, 2, 3)]
+    for copy in tile_sent:
+        copy.start()
+
     @pl.when((z < nz - 1) & (g == 3))
     def _():
         halo_up.start()
+        tile_up.start()
 
     for up in (True, False):
         send_relay("in", 0, sp, up, given("in", 0, g))
@@ -272,7 +318,7 @@
     def _():
         xt[:, 0:HALO, :] = jnp.zeros((2, HALO, xt.shape[2]), xt.dtype)
 
-    docs[0:16, :] = jnp.zeros((16, 128), jnp.float32)
+    docs[0 : 16 + HALO, :] = jnp.zeros((16 + HALO, 128), jnp.float32)
     proj[0:16, :] = jnp.zeros((16, width), proj.dtype)
 
     def spread(block, rx, tx, prx, ptx, sent):
@@ -310,7 +356,6 @@
     def tok_block(side, q):
         return xt.at[side, rows_of(q), :]
 
-    half = 4 * width
     step = 16
     tile = total // 2
     chunk = 32
@@ -333,7 +378,7 @@
                 ).astype(jnp.bfloat16)
             return carry
 
-        lax.fori_loop(0, count // step, body, 0)
+        lax.fori_loop(0, count // step, body, 0, unroll=2)
 
     def load_tokens(j, r):
         h = j // 4
@@ -342,37 +387,24 @@
     def load_acts(j, r):
         return acts[j, r, :]
 
-    def project(l):
+    def add_plane(l, src, first=False):
+        ks = pl.ds(pl.multiple_of(src * 4 * k_in, 4 * k_in), 4 * k_in)
         for m in range(2):
             r = slice(m * tile, (m + 1) * tile)
-
-            def body(i, carry):
-                ks = pl.ds(pl.multiple_of(i * width, width), width)
-                acc[r, :] += jnp.dot(
-                    normed[r, ks], w_in[l, ks, :], preferred_element_type=jnp.float32
-                )
-                return carry
-
-            acc[r, :] = jnp.dot(
-                normed[r, 0:width], w_in[l, 0:width, :], preferred_element_type=jnp.float32
-            )
-            lax.fori_loop(1, 8, body, 0)
-            proj[16 + m * tile : 16 + (m + 1) * tile, :] = acc[r, :].astype(jnp.bfloat16)
-
-    def add_piece(s):
-        ks = pl.ds(pl.multiple_of(s * k_in, k_in), k_in)
-        for m in range(2):
-            r = slice(m * tile, (m + 1) * tile)
-            acc[r, :] += jnp.dot(
-                normed[r, ks], w_in[1, ks, :], preferred_element_type=jnp.float32
-            )
-
-    def add_plane(src):
-        def body(k, carry):
-            add_piece(src * 4 + k)
-            return carry
-
-        lax.fori_loop(0, 4, body, 0)
+            y = jnp.dot(normed[r, ks], w_in[l, ks, :], preferred_element_type=jnp.float32)
+            acc[r, :] = y if first else acc[r, :] + y
+
+    def add_far(l, far):
+        @pl.when(z >= far)
+        def _():
+            add_plane(l, z - far)
+
+        @pl.when(z + far < nz)
+        def _():
+            add_plane(l, z + far)
+
+    def store_proj():
+        proj[16 : 16 + total, :] = acc[...].astype(jnp.bfloat16)
 
     def pool(flags):
         def body(i, carry):
@@ -409,6 +441,7 @@
 
     def mix(part, store):
         l, cols = columns("mix", part, 0)
+        first = (g + 4 * c) * width + cols.start
         for m in range(2):
             r = slice(m * tile, (m + 1) * tile)
             y = jnp.dot(
@@ -418,7 +451,7 @@
                 pooled[1, r, :], w_mix[l, width : 2 * width, cols],
                 preferred_element_type=jnp.float32,
             )
-            store(r, cols, (y * scale[l : l + 1, cols]).astype(jnp.bfloat16))
+            store(r, cols, (y * scale[l : l + 1, pl.ds(pl.multiple_of(first, 128), cols.size)]).astype(jnp.bfloat16))
 
     def normalize_block(k):
         start = pl.multiple_of(HALO + peer_of(g, k) * own, 16)
@@ -432,6 +465,9 @@
         halo_part.start()
         for k in (1, 2, 3):
             halo_peer[k].start()
+        remote(tiles.at[4], tiles.at[4], tile_rx.at[4], tile_rx.at[4], partner).wait_recv()
+        for copy in tile_on:
+            copy.start()
 
     pump_far("in", 0, 1)
     tok_here.wait()
@@ -442,13 +478,14 @@
     spread(tok_block, tok_rx, tok_tx, tok_prx, tok_ptx, tok_sent)
     start_weights("mix", 0)
     start_weights("in", 1)
-    for part in (1, 2, 3):
+    for part in LAST_PARTS:
         start_weights("mix", part)
 
     @pl.when((z > 0) & (g != 3))
     def _():
         remote(halo_here, halo_here, halo.at[0], halo.at[0], partner).wait_recv()
         halo_part.start()
+        remote(tiles.at[4], tiles.at[4], tile_rx.at[4], tile_rx.at[4], partner).wait_recv()
 
     for k in (1, 2):
         from_partner(tok_block, tok_prx, k)
@@ -464,18 +501,40 @@
     pump_plane("mix", 0)
     from_partner(tok_block, tok_prx, 3)
     normalize_block(3)
-    docs[16 : 16 + total, :] = xt[0, :, half : half + 128].astype(jnp.float32)
+    own_tile.wait()
+    for k in (1, 2, 3):
+        spot = tiles.at[peer_of(g, k)]
+        remote(spot, spot, tile_rx.at[peer_of(g, k)], tile_rx.at[peer_of(g, k)], partner).wait_recv()
+
+    def doc_rows(q, lanes):
+        return jnp.broadcast_to(tiles[q, lanes : lanes + 1, :], (128, 128)).T
+
+    for q in range(4):
+        for first in range(0, own, 128):
+            count = min(128, own - first)
+            start = 16 + HALO + q * own + first
+            docs[start : start + count, :] = doc_rows(q, first // 128)[:count]
+
+    @pl.when(z > 0)
+    def _():
+        lead = (own - HALO) % 128
+        docs[16 : 16 + HALO, :] = doc_rows(4, (own - HALO) // 128)[lead : lead + HALO]
+
+    own_weight("in", 0).wait()
+    add_plane(0, z, True)
+    for far in range(1, nz - 1):
+        add_far(0, far)
     pump_far("in", 0, nz - 1)
     for far in range(1, nz - 1):
         pump_far("mix", 0, far)
-    own_weight("in", 0).wait()
-    project(0)
+    add_far(0, nz - 1)
+    store_proj()
     pump_plane("in", 1)
     pool(flags)
     swap_pooled(0).start()
     pump_far("mix", 0, nz - 1)
-    for part in (1, 2, 3):
-        pump_plane("mix", part)
+    for part in LAST_PARTS:
+        pump_own_part(part)
     pooled_arrived(0)
     mine = g + 4 * c
 
@@ -503,28 +562,17 @@
     for k in range(4):
         from_partner(act_block, act_prx, k)
     normalize_rows(1, load_acts, 0, total)
-    acc[...] = jnp.zeros_like(acc)
-    add_plane(z)
+    add_plane(1, z, True)
     for far in range(1, nz - 1):
-        @pl.when(z >= far)
-        def _():
-            add_plane(z - far)
-
-        @pl.when(z + far < nz)
-        def _():
-            add_plane(z + far)
+        add_far(1, far)
 
     @pl.when((z == 0) | (z == nz - 1))
     def _():
-        def body(k, carry):
-            s = (nz - 1 - z) * 4 + peer_of(g, k)
-            arrived("in", 1, s)
-            add_piece(s)
-            return carry
-
-        lax.fori_loop(0, 4, body, 0)
-
-    proj[16 : 16 + total, :] = acc[...].astype(jnp.bfloat16)
+        for k in range(4):
+            arrived("in", 1, (nz - 1 - z) * 4 + peer_of(g, k))
+        add_plane(1, nz - 1 - z)
+
+    store_proj()
     swap_pooled(0).wait_send()
     pool(flags)
     swap_pooled(1).start()
@@ -540,8 +588,18 @@
             return pltpu.make_async_copy(src, dst, out_rx.at[part, 0])
         return remote(src, dst, out_tx.at[part, k], out_rx.at[part, k], peer(k))
 
-    for part in (1, 2, 3):
-        pump_line("mix", part)
+    inside = (z > 0) & (z < nz - 1)
+
+    @pl.when(inside)
+    def _():
+        for part in LAST_PARTS:
+            far_parts(part)
+
+    for part in LAST_PARTS:
+        @pl.when(jnp.logical_not(inside))
+        def _():
+            far_parts(part)
+
         if part == 1:
             pooled_arrived(1)
         mix(part, store_last)
@@ -553,6 +611,8 @@
         for l in range(2 if kind == "in" else len(PARTS)):
             for k in (1, 2, 3):
                 give_weight(kind, l, k).wait_send()
+            if kind == "mix" and l:
+                continue
             for src in range(nz):
                 for k in range(4):
                     s = src * 4 + k
@@ -565,9 +625,23 @@
                     def _():
                         relay(kind, l, s, False).wait_send()
 
+    for part in LAST_PARTS:
+        for src in range(nz):
+            @pl.when((z >= src) & (z < nz - 1))
+            def _():
+                plane_relay(part, src, True).wait_send()
+
+            @pl.when((z <= src) & (z > 0))
+            def _():
+                plane_relay(part, src, False).wait_send()
+
+    for copy in tile_sent:
+        copy.wait_send()
+
     @pl.when((z < nz - 1) & (g == 3))
     def _():
         halo_up.wait_send()
+        tile_up.wait_send()
 
     @pl.when(z > 0)
     def _():
@@ -577,10 +651,12 @@
         def _():
             for k in (1, 2, 3):
                 halo_peer[k].wait_send()
+            for copy in tile_on:
+                copy.wait_send()
 
     for copy in tok_sent + act_sent:
         copy.wait_send()
-    for part in (1, 2, 3):
+    for part in LAST_PARTS:
         for k in (1, 2, 3):
             _, place = columns("mix", part, peer_of(g, k))
             _, cols = columns("mix", part, 0)
@@ -597,16 +673,14 @@
     nsp = lax.axis_size("sp")
     nz = nsp // 4
     total = HALO + 4 * own
-    tile_docs = jnp.broadcast_to((doc_ids + 1).astype(jnp.bfloat16)[:, None], (own, 128))
-    tok = jnp.concatenate([tokens, tile_docs], axis=1)
-    block = lax.axis_index("sp") % 4 + 4 * lax.axis_index("tp")
-    scale = lax.dynamic_slice_in_dim(out_scale, block * width, width, 1)
+    numbers = (doc_ids + 1).astype(jnp.float32)
+    doc_tile = jnp.pad(numbers, (0, 8 * 128 - own)).reshape(8, 128)
     any_spec = pl.BlockSpec(memory_space=pl.ANY)
     vmem_spec = pl.BlockSpec(memory_space=pltpu.VMEM)
     bf16, f32 = jnp.bfloat16, jnp.float32
     dma = pltpu.SemaphoreType.DMA
     scratch = [
-        pltpu.VMEM((2, total, local_width + 128), bf16),
+        pltpu.VMEM((2, total, local_width), bf16),
         pltpu.VMEM((total, 8 * width), bf16),
         pltpu.VMEM((8, total, width), bf16),
         pltpu.VMEM((2, 8 * width, width), bf16),
@@ -619,19 +693,20 @@
     ]
     parts = len(PARTS)
     scratch += [dma((n, nsp)) for _ in range(3) for n in (2, parts)]
-    scratch += [dma((2, 4)), dma((parts, 4))]
+    scratch += [dma((2, 4)), dma((parts, 4)), dma((parts, 4))]
+    scratch += [pltpu.VMEM((5, 8, 128), f32), dma((5,)), dma((7,))]
     scratch += [dma((5,)) for _ in range(4)] + [dma((2,)), dma((5,))]
     scratch += [dma((5,)) for _ in range(4)] + [dma((2, 2)), dma((parts, 4)), dma((parts, 4))]
     return pl.pallas_call(
         functools.partial(fused_kernel, nz, own),
         out_shape=jax.ShapeDtypeStruct((own, local_width), bf16),
-        in_specs=[any_spec, any_spec, any_spec, vmem_spec, vmem_spec],
+        in_specs=[any_spec, vmem_spec, any_spec, any_spec, vmem_spec, vmem_spec],
         out_specs=any_spec,
         scratch_shapes=scratch,
         compiler_params=pltpu.CompilerParams(
             collective_id=0, has_side_effects=True, vmem_limit_bytes=60 * 1024 * 1024
         ),
-    )(tok, in_proj, mix_proj, norm_gain, scale)
+    )(tokens, doc_tile, in_proj, mix_proj, norm_gain, out_scale)
 
 
 def solution(mesh):

time: 203 us -> 195 us (0.961)
  Pallas kernels: 196 us -> 191 us
  other arithmetic: 3.11 us -> 0.68 us
    pallas_call x1, Pallas kernels: 196 us -> 191 us  [fused_shards(): pl.pallas_call(functools.partial(fused_kernel, nz, own), out_shape=jax.Sh...]
    concatenate x1 -> x0, other arithmetic: 2.42 us -> none  [fused_shards(): tok = jnp.concatenate([tokens, tile_docs], axis=1)]
where the time goes in v3:
time: 195 us
  Pallas kernels  191 us (98%)
  local copies, waits for them, and re-layouts  3.01 us (2%)
    pallas_call x1, Pallas kernels, fused_shards(): pl.pallas_call(functools.partial(fused_kernel, nz, own), out_shape=jax.Sh...  191 us

profile of v3, /device:TPU:0, one launch (start us, length us, event | category | flops | bytes accessed | tf_op | source)
XLA Modules:
  0.0 194.7 jit_solution(13612404472415072863)
XLA Ops:
  0.0 0.7 add_convert_fusion
  0.7 0.6 pad_bitcast_fusion.doc_tile
  1.3 191.0 %shard_map.64 = bf16[288,2048]{1,0:T(8,128)(2,1)} custom-call(bf16[288,2048]{1,0:T(8,128)(2,1)} %tok.1, f32[8,128]{1,0:T(8,128)} %pad_bitcast_fusion.doc_tile, bf16[2,256,2048]{2,1,0:T(8,128)(2,1)} %in_w.1, bf16[2,64,2048]{2,1,0:T(8,128)(2,1)} %mix_w.1, f32[2,4096]{1,0:T(2,128)} %gain.1, f32[2,4096]{1,0:T(2,128)} %scale.1), custom_call_target="tpu_custom_call" | custom-call | tf_op jit(solution)/shard_map/pallas_call | solution.py:700
  192.3 2.4 %copy.8 = bf16[288,2048]{1,0:T(8,128)(2,1)} copy(bf16[288,2048]{1,0:T(8,128)(2,1)} %shard_map.64) | data formatting | bytes 2359296

commit v4 on v3

--- a/solution.py
+++ b/solution.py
@@ -304,6 +304,7 @@
     for up in (True, False):
         send_relay("in", 0, sp, up, given("in", 0, g))
     start_weights("in", 0)
+    start_weights("mix", 0)
     tok_here = pltpu.make_async_copy(tok, xt.at[c, rows_of(g), :], tok_rx.at[0])
     tok_here.start()
     tok_sent = [remote(tok, xt.at[c, rows_of(g), :], tok_ptx.at[0], tok_prx.at[0], partner)]
@@ -394,6 +395,20 @@
             y = jnp.dot(normed[r, ks], w_in[l, ks, :], preferred_element_type=jnp.float32)
             acc[r, :] = y if first else acc[r, :] + y
 
+    def add_last(l):
+        @pl.when((z == 0) | (z == nz - 1))
+        def _():
+            src = nz - 1 - z
+            ks = pl.ds(pl.multiple_of(src * 4 * k_in, 4 * k_in), 4 * k_in)
+            for m in range(2):
+                r = slice(m * tile, (m + 1) * tile)
+                y = jnp.dot(normed[r, ks], w_in[l, ks, :], preferred_element_type=jnp.float32)
+                proj[16 + m * tile : 16 + (m + 1) * tile, :] = (acc[r, :] + y).astype(jnp.bfloat16)
+
+        @pl.when((z > 0) & (z < nz - 1))
+        def _():
+            store_proj()
+
     def add_far(l, far):
         @pl.when(z >= far)
         def _():
@@ -406,44 +421,52 @@
     def store_proj():
         proj[16 : 16 + total, :] = acc[...].astype(jnp.bfloat16)
 
-    def pool(flags):
+    split = total // 2 // chunk * chunk + chunk
+    spans = ((0, split), (split, total - split))
+
+    def pool(flags, first, count):
         def body(i, carry):
-            base = pl.multiple_of(i * chunk, chunk)
+            base = pl.multiple_of(first + i * chunk, chunk)
             ext = pl.ds(base, chunk + 16)
             d = docs[ext, :]
             same = []
-            count = jnp.ones_like(d)
+            tally = jnp.ones_like(d)
             for j in range(4):
                 ok = jnp.where(pltpu.roll(d, 2**j, 0) == d, flags[j], 0.0)
                 same.append(ok)
-                count = count + ok * pltpu.roll(count, 2**j, 0)
+                tally = tally + ok * pltpu.roll(tally, 2**j, 0)
+            share = 1.0 / tally
             for q in range(width // 128):
                 cols = slice(q * 128, (q + 1) * 128)
                 p = proj[ext, cols].astype(jnp.float32)
                 total_sum = p
                 for j in range(4):
                     total_sum = total_sum + same[j] * pltpu.roll(total_sum, 2**j, 0)
-                v = total_sum / count - p
+                v = total_sum * share - p
                 pooled[c, pl.ds(base, chunk), cols] = v[16:, :].astype(jnp.bfloat16)
             return carry
 
-        lax.fori_loop(0, total // chunk, body, 0)
+        lax.fori_loop(0, count // chunk, body, 0)
 
     flags = [jnp.where(g >= j, jnp.float32(1.0), jnp.float32(0.0)) for j in range(4)]
 
-    def swap_pooled(l):
-        here = pooled.at[c]
-        return remote(here, here, pool_sem.at[l, 0], pool_sem.at[l, 1], partner)
-
-    def pooled_arrived(l):
-        there = pooled.at[1 - c]
-        remote(there, there, pool_sem.at[l, 1], pool_sem.at[l, 1], partner).wait_recv()
-
-    def mix(part, store):
+    def swap_pooled(l, h):
+        here = pooled.at[c, pl.ds(*spans[h]), :]
+        return remote(here, here, pool_sem.at[l, h], pool_sem.at[l, 2 + h], partner)
+
+    def pooled_arrived(l, h):
+        there = pooled.at[1 - c, pl.ds(*spans[h]), :]
+        remote(there, there, pool_sem.at[l, 2 + h], pool_sem.at[l, 2 + h], partner).wait_recv()
+
+    def pool_and_swap(l):
+        for h in range(2):
+            pool(flags, *spans[h])
+            swap_pooled(l, h).start()
+
+    def mix(part, spans, store):
         l, cols = columns("mix", part, 0)
         first = (g + 4 * c) * width + cols.start
-        for m in range(2):
-            r = slice(m * tile, (m + 1) * tile)
+        for r in spans:
             y = jnp.dot(
                 pooled[0, r, :], w_mix[l, 0:width, cols], preferred_element_type=jnp.float32
             )
@@ -458,6 +481,7 @@
         normalize_rows(0, load_tokens, start, own)
 
     pump_plane("in", 0)
+    pump_plane("mix", 0)
 
     @pl.when((z > 0) & (g == 3))
     def _():
@@ -470,13 +494,14 @@
             copy.start()
 
     pump_far("in", 0, 1)
+    pump_far("mix", 0, 1)
     tok_here.wait()
     from_partner(tok_block, tok_prx, 0)
     normalize_block(0)
     for far in range(2, nz - 1):
         pump_far("in", 0, far)
+        pump_far("mix", 0, far)
     spread(tok_block, tok_rx, tok_tx, tok_prx, tok_ptx, tok_sent)
-    start_weights("mix", 0)
     start_weights("in", 1)
     for part in LAST_PARTS:
         start_weights("mix", part)
@@ -498,7 +523,6 @@
 
     normalize_rows(0, load_tokens, 0, HALO)
     spread_end(tok_block, tok_rx, tok_prx, tok_ptx, tok_sent)
-    pump_plane("mix", 0)
     from_partner(tok_block, tok_prx, 3)
     normalize_block(3)
     own_tile.wait()
@@ -525,23 +549,25 @@
     for far in range(1, nz - 1):
         add_far(0, far)
     pump_far("in", 0, nz - 1)
-    for far in range(1, nz - 1):
-        pump_far("mix", 0, far)
-    add_far(0, nz - 1)
-    store_proj()
+    add_last(0)
     pump_plane("in", 1)
-    pool(flags)
-    swap_pooled(0).start()
+    pool_and_swap(0)
     pump_far("mix", 0, nz - 1)
-    for part in LAST_PARTS:
-        pump_own_part(part)
-    pooled_arrived(0)
+    inside = (z > 0) & (z < nz - 1)
+
+    @pl.when(jnp.logical_not(inside))
+    def _():
+        for part in LAST_PARTS:
+            pump_own_part(part)
+
+    for h in range(2):
+        pooled_arrived(0, h)
     mine = g + 4 * c
 
     def store_acts(r, cols, v):
         acts[mine, r, cols] = v
 
-    mix(0, store_acts)
+    mix(0, [slice(m * tile, (m + 1) * tile) for m in range(2)], store_acts)
     here = acts.at[mine]
     act_sent = [remote(here, here, act_ptx.at[0], act_prx.at[0], partner)]
     for k in (1, 2):
@@ -559,6 +585,12 @@
     for far in range(2, nz - 1):
         pump_far("in", 1, far, range(2, 4))
     spread_end(act_block, act_rx, act_prx, act_ptx, act_sent)
+
+    @pl.when(inside)
+    def _():
+        for part in LAST_PARTS:
+            pump_own_part(part)
+
     for k in range(4):
         from_partner(act_block, act_prx, k)
     normalize_rows(1, load_acts, 0, total)
@@ -570,12 +602,16 @@
     def _():
         for k in range(4):
             arrived("in", 1, (nz - 1 - z) * 4 + peer_of(g, k))
-        add_plane(1, nz - 1 - z)
-
-    store_proj()
-    swap_pooled(0).wait_send()
-    pool(flags)
-    swap_pooled(1).start()
+
+    add_last(1)
+    for h in range(2):
+        swap_pooled(0, h).wait_send()
+    pool_and_swap(1)
+    @pl.when(inside)
+    def _():
+        for part in LAST_PARTS:
+            far_parts(part)
+
     def store_last(r, cols, v):
         last[r, cols] = v
 
@@ -588,25 +624,21 @@
             return pltpu.make_async_copy(src, dst, out_rx.at[part, 0])
         return remote(src, dst, out_tx.at[part, k], out_rx.at[part, k], peer(k))
 
-    inside = (z > 0) & (z < nz - 1)
-
-    @pl.when(inside)
-    def _():
-        for part in LAST_PARTS:
-            far_parts(part)
-
     for part in LAST_PARTS:
         @pl.when(jnp.logical_not(inside))
         def _():
             far_parts(part)
 
         if part == 1:
-            pooled_arrived(1)
-        mix(part, store_last)
-        for k in (1, 2, 3, 0):
+            for h in range(2):
+                pooled_arrived(1, h)
+        for k in (3, 1, 2, 0):
+            start = pl.multiple_of(HALO + peer_of(g, k) * own, 16)
+            mix(part, [pl.ds(start, own)], store_last)
             out_copy(part, k).start()
 
-    swap_pooled(1).wait_send()
+    for h in range(2):
+        swap_pooled(1, h).wait_send()
     for kind in ("in", "mix"):
         for l in range(2 if kind == "in" else len(PARTS)):
             for k in (1, 2, 3):
@@ -696,7 +728,7 @@
     scratch += [dma((2, 4)), dma((parts, 4)), dma((parts, 4))]
     scratch += [pltpu.VMEM((5, 8, 128), f32), dma((5,)), dma((7,))]
     scratch += [dma((5,)) for _ in range(4)] + [dma((2,)), dma((5,))]
-    scratch += [dma((5,)) for _ in range(4)] + [dma((2, 2)), dma((parts, 4)), dma((parts, 4))]
+    scratch += [dma((5,)) for _ in range(4)] + [dma((2, 4)), dma((parts, 4)), dma((parts, 4))]
     return pl.pallas_call(
         functools.partial(fused_kernel, nz, own),
         out_shape=jax.ShapeDtypeStruct((own, local_width), bf16),

time: 195 us -> 193 us (0.990)
  Pallas kernels: 191 us -> 189 us
where the time goes in v4:
time: 193 us
  Pallas kernels  189 us (98%)
  local copies, waits for them, and re-layouts  3.01 us (2%)
    pallas_call x1, Pallas kernels, fused_shards(): pl.pallas_call(functools.partial(fused_kernel, nz, own), out_shape=jax.Sh...  189 us

profile of v4, /device:TPU:0, one launch (start us, length us, event | category | flops | bytes accessed | tf_op | source)
XLA Modules:
  0.0 193.0 jit_solution(11094960849411733161)
XLA Ops:
  0.0 0.7 add_convert_fusion
  0.7 0.6 pad_bitcast_fusion.doc_tile
  1.3 189.3 %shard_map.64 = bf16[288,2048]{1,0:T(8,128)(2,1)} custom-call(bf16[288,2048]{1,0:T(8,128)(2,1)} %tok.1, f32[8,128]{1,0:T(8,128)} %pad_bitcast_fusion.doc_tile, bf16[2,256,2048]{2,1,0:T(8,128)(2,1)} %in_w.1, bf16[2,64,2048]{2,1,0:T(8,128)(2,1)} %mix_w.1, f32[2,4096]{1,0:T(2,128)} %gain.1, f32[2,4096]{1,0:T(2,128)} %scale.1), custom_call_target="tpu_custom_call" | custom-call | tf_op jit(solution)/shard_map/pallas_call | solution.py:732
  190.6 2.4 %copy.8 = bf16[288,2048]{1,0:T(8,128)(2,1)} copy(bf16[288,2048]{1,0:T(8,128)(2,1)} %shard_map.64) | data formatting | bytes 2359296

commit v5 on v4

--- a/solution.py
+++ b/solution.py
@@ -578,12 +578,19 @@
     def act_block(side, q):
         return acts.at[q + 4 * side]
 
-    pump_far("in", 1, 1)
-    for far in range(2, nz - 1):
-        pump_far("in", 1, far, range(2))
+    @pl.when(inside)
+    def _():
+        pump_far("in", 1, 1)
+        for far in range(2, nz - 1):
+            pump_far("in", 1, far, range(2))
+
     spread(act_block, act_rx, act_tx, act_prx, act_ptx, act_sent)
-    for far in range(2, nz - 1):
-        pump_far("in", 1, far, range(2, 4))
+
+    @pl.when(inside)
+    def _():
+        for far in range(2, nz - 1):
+            pump_far("in", 1, far, range(2, 4))
+
     spread_end(act_block, act_rx, act_prx, act_ptx, act_sent)
 
     @pl.when(inside)
@@ -594,6 +601,11 @@
     for k in range(4):
         from_partner(act_block, act_prx, k)
     normalize_rows(1, load_acts, 0, total)
+    @pl.when(jnp.logical_not(inside))
+    def _():
+        for far in range(1, nz - 1):
+            pump_far("in", 1, far)
+
     add_plane(1, z, True)
     for far in range(1, nz - 1):
         add_far(1, far)

time: 193 us -> 193 us (level)
  no operation moved by 1% of the time
where the time goes in v5:
time: 193 us
  Pallas kernels  189 us (98%)
  local copies, waits for them, and re-layouts  3.01 us (2%)
    pallas_call x1, Pallas kernels, fused_shards(): pl.pallas_call(functools.partial(fused_kernel, nz, own), out_shape=jax.Sh...  189 us

profile of v5, /device:TPU:0, one launch (start us, length us, event | category | flops | bytes accessed | tf_op | source)
XLA Modules:
  0.0 193.0 jit_solution(16271605836135044763)
XLA Ops:
  0.0 0.7 add_convert_fusion
  0.7 0.6 pad_bitcast_fusion.doc_tile
  1.3 189.3 %shard_map.64 = bf16[288,2048]{1,0:T(8,128)(2,1)} custom-call(bf16[288,2048]{1,0:T(8,128)(2,1)} %tok.1, f32[8,128]{1,0:T(8,128)} %pad_bitcast_fusion.doc_tile, bf16[2,256,2048]{2,1,0:T(8,128)(2,1)} %in_w.1, bf16[2,64,2048]{2,1,0:T(8,128)(2,1)} %mix_w.1, f32[2,4096]{1,0:T(2,128)} %gain.1, f32[2,4096]{1,0:T(2,128)} %scale.1), custom_call_target="tpu_custom_call" | custom-call | tf_op jit(solution)/shard_map/pallas_call | solution.py:744
  190.6 2.4 %copy.8 = bf16[288,2048]{1,0:T(8,128)(2,1)} copy(bf16[288,2048]{1,0:T(8,128)(2,1)} %shard_map.64) | data formatting | bytes 2359296
